TPU v7x, 32 devices: a whole 2x2x4 slice. The times are simulated.
32 devices in a mesh: sp: 8 (over z, y), tp: 4 (over x, core).
Axes of the slice: x: 2, y: 2, z: 4, core: 2. Of those that a mesh axis runs over, the one named last changes fastest.
Arguments:
- queries: bfloat16 [6144, 1536], P('sp', 'tp'), may hold values from -130 to 130, as said below
- keys: bfloat16 [6144, 512], P('sp', 'tp'), may hold values from -6 to 6
- values: bfloat16 [6144, 512], P('sp', 'tp'), may hold values from -6 to 6
- residual: bfloat16 [6144, 2048], P(('sp', 'tp')), may hold values from -6 to 6
- sinks: float32 [12], P('tp'), may hold values from 2 to 6
- out_weight: bfloat16 [1536, 2048], P('tp'), may hold values from -0.15625 to 0.15625
- up_weight: bfloat16 [2048, 8192], P('sp', 'tp'), may hold values from -0.125 to 0.125
- down_weight: bfloat16 [8192, 2048], P('tp', 'sp'), may hold values from -0.0625 to 0.0625
- gains: float32 [2, 2048], replicated, may hold values from 0.1 to 1.9
- biases: float32 [2, 2048], replicated, may hold values from -3 to 3
Outputs:
- layer_out: bfloat16 [6144, 2048], P(('sp', 'tp'))
Inputs may be any that keep to these rules, and one draw needn't show every extreme that they name: `queries`: entries of order one, with some rows far larger in some draws.
All inputs are finite; a program needn't handle non-finite values.
Results may differ from a plain program's by a relative error of at most 0.0095.
Values may be sent and summed in bfloat16 or wider, within the bound.
A program may use at most 128 MiB of HBM per device.

v0:
```python
import jax
import jax.numpy as jnp
from jax import lax
from jax.sharding import PartitionSpec as P

HEADS = 12
HEAD = 128
WINDOW = 128
deep_alpha = 1.6817928
norm_eps = 1e-05
neg_big = -1e30


def from_behind(block, axis, distance):
    devices = range(lax.axis_size(axis))
    route = [(i - distance, i) for i in devices if i - distance in devices]
    return lax.ppermute(block, axis, route)


def layer_norm(stream, gain, bias):
    mean = jnp.mean(stream, axis=-1, keepdims=True)
    spread = jnp.mean(jnp.square(stream - mean), axis=-1, keepdims=True)
    return ((stream - mean) * lax.rsqrt(spread + norm_eps) * gain + bias).astype(jnp.bfloat16)


def attend(queries, keys, values, before, sinks, offset, rank_tp):
    tokens = keys.shape[0]
    kv_local = keys.shape[1] // HEAD
    heads_local = sinks.shape[0]
    group = heads_local // kv_local
    blocks = tokens // WINDOW
    q_blocks = queries.reshape(blocks, WINDOW, kv_local, group, HEAD)
    key_ext = jnp.concatenate([before[0], keys], axis=0).reshape(tokens + WINDOW, kv_local, HEAD)
    val_ext = jnp.concatenate([before[1], values], axis=0).reshape(tokens + WINDOW, kv_local, HEAD)
    key_win = jnp.concatenate(
        [
            key_ext[:tokens].reshape(blocks, WINDOW, kv_local, HEAD),
            key_ext[WINDOW:].reshape(blocks, WINDOW, kv_local, HEAD),
        ],
        axis=1,
    )
    val_win = jnp.concatenate(
        [
            val_ext[:tokens].reshape(blocks, WINDOW, kv_local, HEAD),
            val_ext[WINDOW:].reshape(blocks, WINDOW, kv_local, HEAD),
        ],
        axis=1,
    )
    logits = jnp.einsum(
        "nqkgd,nskd->nkgqs", q_blocks, key_win, preferred_element_type=jnp.float32
    ) * HEAD ** (-0.5)
    q_index = jnp.arange(WINDOW, dtype=jnp.int32)[:, None]
    k_index = jnp.arange(2 * WINDOW, dtype=jnp.int32)[None, :]
    dist = q_index + WINDOW - k_index
    block_id = jnp.arange(blocks, dtype=jnp.int32)[:, None, None]
    key_pos = offset + block_id * WINDOW - WINDOW + k_index
    valid = (dist >= 0) & (dist < WINDOW) & (key_pos >= 0)
    heads = (jnp.arange(heads_local, dtype=jnp.int32) + rank_tp * heads_local).astype(jnp.float32)
    slopes = jnp.exp2(-8.0 * (heads + 1.0) / HEADS).reshape(kv_local, group)[:, :, None, None]
    logits = logits - slopes * dist.astype(jnp.float32)
    logits = jnp.where(valid[:, None, None], logits, neg_big)
    sink = sinks.reshape(kv_local, group)[:, :, None, None]
    top = jnp.maximum(jnp.max(logits, axis=-1, keepdims=True), sink)
    probs = jnp.exp(logits - top)
    denom = jnp.sum(probs, axis=-1, keepdims=True) + jnp.exp(sink - top)
    weight = (probs / denom).astype(jnp.bfloat16)
    attended = jnp.einsum("nkgqs,nskd->nqkgd", weight, val_win, preferred_element_type=jnp.float32)
    return attended.astype(jnp.bfloat16).reshape(tokens, heads_local * HEAD)


def on_device(
    queries, keys, values, residual, sinks, out_weight, up_weight, down_weight, gains, biases
):
    tokens = queries.shape[0]
    rank_tp = lax.axis_index("tp")
    up_full, down_full = (
        lax.all_gather(up_weight, "sp", axis=0, tiled=True),
        lax.all_gather(down_weight, "sp", axis=1, tiled=True),
    )
    tails = jnp.stack([keys[tokens - WINDOW :], values[tokens - WINDOW :]])
    before = from_behind(tails, "sp", 1)
    offset = lax.axis_index("sp") * tokens
    attended = attend(queries, keys, values, before, sinks, offset, rank_tp)
    mix = lax.psum_scatter(
        jnp.dot(attended, out_weight, preferred_element_type=jnp.float32).astype(jnp.bfloat16),
        "tp",
        scatter_dimension=0,
        tiled=True,
    ).astype(jnp.float32)
    normed = layer_norm(deep_alpha * residual.astype(jnp.float32) + mix, gains[0], biases[0])
    whole = lax.all_gather(normed, "tp", axis=0, tiled=True)
    upward = jnp.dot(whole, up_full, preferred_element_type=jnp.float32)
    act = jnp.square(jax.nn.relu(upward)).astype(jnp.bfloat16)
    terms = jnp.dot(act, down_full, preferred_element_type=jnp.float32)
    ffn = lax.psum_scatter(
        terms.astype(jnp.bfloat16), "tp", scatter_dimension=0, tiled=True
    ).astype(jnp.float32)
    return layer_norm(deep_alpha * normed.astype(jnp.float32) + ffn, gains[1], biases[1])


def solution(mesh):
    return jax.shard_map(
        on_device,
        mesh=mesh,
        in_specs=(
            P("sp", "tp"),
            P("sp", "tp"),
            P("sp", "tp"),
            P(("sp", "tp"), None),
            P("tp"),
            P("tp", None),
            P("sp", "tp"),
            P("tp", "sp"),
            P(),
            P(),
        ),
        out_specs=P(("sp", "tp"), None),
        check_vma=False,
    )
```

profile of v0, /device:TPU:0, one launch (start us, length us, event | category | flops | bytes accessed | tf_op | source)
XLA Modules:
  0.0 408.7 jit_solution(9440139312392734191)
XLA Ops:
  6.5 0.9 slice_bitcast_fusion.2
  7.5 0.6 pad_maximum_fusion.2
  8.1 5.5 %collective-permute-start = (bf16[2,128,128]{2,1,0:T(8,128)(2,1)}, bf16[2,128,128]{2,1,0:T(8,128)(2,1)}, u32[]{:S(2)}, u32[]{:S(2)}) collective-permute-start(bf16[2,128,128]{2,1,0:T(8,128)(2,1)} %pad_maximum_fusion.2), channel_id=1, source_target_pairs={{0,4},{4,8},{8,12},{12,16},{16,20},{20,24},{24,28},{1,5},{5,9},{9,... | collective-permute-start | bytes 196616 | tf_op jit(solution)/shard_map/ppermute | solution.py:17
  13.9 1.0 broadcast_and_fusion
  15.3 0.8 slice_bitcast_fusion.1
  16.1 0.9 pad_maximum_fusion
  17.0 1.7 fusion.21
  18.8 1.3 copy-done.5
  20.7 2.2 fusion.2
  23.3 3.5 convolution_convert_fusion.1
  26.9 0.6 copy-done.8
  27.6 39.3 %reduce-scatter.3.cloned.1.call-done = bf16[192,2048]{1,0:T(8,128)(2,1)} async-done(((bf16[768,2048]{1,0:T(8,128)(2,1)}), bf16[192,2048]{1,0:T(8,128)(2,1)}) %reduce-scatter.3.cloned.1.call-update) | async-done | bytes 786448 | tf_op jit(solution)/shard_map/reduce_scatter | solution.py:84
  66.9 1.5 fusion.3
  69.0 1.4 add_convert_fusion.1
  70.4 0.7 all-gather.6.cloned.1.call-update
  71.1 0.5 all-gather.8.cloned.1.call-update
  71.9 27.1 %all-gather.4.cloned.1.call-done = bf16[768,2048]{1,0:T(8,128)(2,1)} async-done(((bf16[192,2048]{1,0:T(8,128)(2,1)}), bf16[768,2048]{1,0:T(8,128)(2,1)}) %all-gather.4.cloned.1.call-update) | async-done | bytes 3145744 | tf_op jit(solution)/shard_map/all_gather | solution.py:91
  99.0 126.6 %all-gather.6.cloned.1.call-done = bf16[2048,2048]{1,0:T(8,128)(2,1)} async-done(((bf16[256,2048]{1,0:T(8,128)(2,1)}), bf16[2048,2048]{1,0:T(8,128)(2,1)}) %all-gather.6.cloned.1.call-update) | async-done | bytes 8388624 | tf_op jit(solution)/shard_map/all_gather | solution.py:77
  225.6 11.9 %multiply_convert_fusion = bf16[768,2048]{1,0:T(8,128)(2,1)} fusion(bf16[768,2048]{1,0:T(8,128)(2,1)} %all-gather.4.cloned.1.call-done, bf16[2048,2048]{1,0:T(8,128)(2,1)} %all-gather.6.cloned.1.call-done), kind=kOutput, calls=%fused_computation | convolution fusion | flops 6447169536 | bytes 14680064 | tf_op jit(solution)/shard_map/dot_general | solution.py:92
  237.5 113.2 %all-gather.8.cloned.1.call-done = bf16[2048,2048]{1,0:T(8,128)(2,1)} async-done(((bf16[2048,256]{1,0:T(8,128)(2,1)}), bf16[2048,2048]{1,0:T(8,128)(2,1)}) %all-gather.8.cloned.1.call-update) | async-done | bytes 8388624 | tf_op jit(solution)/shard_map/all_gather | solution.py:78
  350.7 11.8 %convolution_convert_fusion = bf16[768,2048]{1,0:T(8,128)(2,1)} fusion(bf16[768,2048]{1,0:T(8,128)(2,1)} %multiply_convert_fusion, bf16[2048,2048]{1,0:T(8,128)(2,1)} %all-gather.8.cloned.1.call-done), kind=kOutput, calls=%fused_computation.1 | convolution fusion | flops 6444023808 | bytes 14680064 | tf_op jit(solution)/shard_map/dot_general | solution.py:94
  362.6 36.2 %reduce-scatter.5.cloned.1.call-done = bf16[192,2048]{1,0:T(8,128)(2,1)} async-done(((bf16[768,2048]{1,0:T(8,128)(2,1)}), bf16[192,2048]{1,0:T(8,128)(2,1)}) %reduce-scatter.5.cloned.1.call-update) | async-done | bytes 786448 | tf_op jit(solution)/shard_map/reduce_scatter | solution.py:95
  398.8 1.5 fusion.4
  400.8 1.4 add_convert_fusion
  (52 shorter events, 3.1 us)
Async XLA Ops:
  6.5 16.8 %copy-start = (bf16[384,2048]{1,0:T(8,128)(2,1)S(1)}, bf16[384,2048]{1,0:T(8,128)(2,1)}, u32[]{:S(2)}) copy-start(bf16[384,2048]{1,0:T(8,128)(2,1)} %param.15) | copy-start | bytes 4718596
  6.5 8.5 %copy-start.6 = (bf16[768,128]{1,0:T(8,128)(2,1)S(1)}, bf16[768,128]{1,0:T(8,128)(2,1)}, u32[]{:S(2)}) copy-start(bf16[768,128]{1,0:T(8,128)(2,1)} %param.12) | copy-start | bytes 589828
  6.5 8.3 %copy-start.7 = (bf16[768,384]{1,0:T(8,128)(2,1)S(1)}, bf16[768,384]{1,0:T(8,128)(2,1)}, u32[]{:S(2)}) copy-start(bf16[768,384]{1,0:T(8,128)(2,1)} %param.10) | copy-start | bytes 1769476
  6.5 60.4 %reduce-scatter.3.cloned.1.call-start = ((), (), s32[]{:S(2)}) async-start(), calls=%async_computation.2 | async-start | bytes 3932160 | tf_op jit(solution)/shard_map/reduce_scatter | solution.py:84
  8.1 7.1 %collective-permute-start = (bf16[2,128,128]{2,1,0:T(8,128)(2,1)}, bf16[2,128,128]{2,1,0:T(8,128)(2,1)}, u32[]{:S(2)}, u32[]{:S(2)}) collective-permute-start(bf16[2,128,128]{2,1,0:T(8,128)(2,1)} %pad_maximum_fusion.2), channel_id=1, source_target_pairs={{0,4},{4,8},{8,12},{12,16},{16,20},{20,24},{24,28},{1,5},{5,9},{9,... | collective-permute-start | bytes 196616 | tf_op jit(solution)/shard_map/ppermute | solution.py:17
  17.0 1.7 copy-start.10
  18.7 1.4 copy-start.5
  26.8 0.7 copy-start.8
  26.8 0.7 copy-start.9
  26.8 40.1 %copy-start.2 = (bf16[192,2048]{1,0:T(8,128)(2,1)S(1)}, bf16[192,2048]{1,0:T(8,128)(2,1)}, u32[]{:S(2)}) copy-start(bf16[192,2048]{1,0:T(8,128)(2,1)} %param.13) | copy-start | bytes 2359300
  26.9 72.1 %all-gather.4.cloned.1.call-start = ((), (), s32[]{:S(2)}) async-start(), calls=%async_computation.3 | async-start | bytes 3932160 | tf_op jit(solution)/shard_map/all_gather | solution.py:91
  66.9 1.6 copy-start.3
  70.3 155.3 %all-gather.6.cloned.1.call-start = ((), (), s32[]{:S(2)}) async-start(), calls=%async_computation.4 | async-start | bytes 9437184 | tf_op jit(solution)/shard_map/all_gather | solution.py:77
  71.1 279.6 %all-gather.8.cloned.1.call-start = ((), (), s32[]{:S(2)}) async-start(), calls=%async_computation.5 | async-start | bytes 9437184 | tf_op jit(solution)/shard_map/all_gather | solution.py:78
  71.7 327.1 %reduce-scatter.5.cloned.1.call-start = ((), (), s32[]{:S(2)}) async-start(), calls=%async_computation.6 | async-start | bytes 3932160 | tf_op jit(solution)/shard_map/reduce_scatter | solution.py:95
  362.5 36.2 %copy-start.1 = (bf16[192,2048]{1,0:T(8,128)(2,1)S(1)}, bf16[192,2048]{1,0:T(8,128)(2,1)}, u32[]{:S(2)}) copy-start(bf16[192,2048]{1,0:T(8,128)(2,1)} %add_convert_fusion.1) | copy-start | bytes 2359300
  398.8 1.6 copy-start.4
Sparse Core Ops, SparseCore 0:
  27.0 39.9 reduce-scatter.2
  70.5 28.4 all-gather.3
  101.1 124.4 all-gather.5
  227.5 123.1 all-gather.7
  362.7 36.0 reduce-scatter.4
where the time goes:
time: 409 us
  waiting for transfers between devices  344 us (84%)
  matrix products  31.1 us (8%)
  between operations  13.3 us (3%)
  other arithmetic  10 us (2%)
  starting transfers between devices  5.86 us (1%)
  local copies, waits for them, and re-layouts  4.69 us (1%)
    all_gather x1, waiting for transfers between devices, on_device(): lax.all_gather(up_weight, 'sp', axis=0, tiled=True)  127 us
    all_gather x1, waiting for transfers between devices, on_device(): lax.all_gather(down_weight, 'sp', axis=1, tiled=True)  113 us
    reduce_scatter x1, waiting for transfers between devices, on_device(): lax.psum_scatter(jnp.dot(attended, out_weight, preferred_element_type=jnp...  39.3 us
    reduce_scatter x1, waiting for transfers between devices, on_device(): lax.psum_scatter(terms.astype(jnp.bfloat16), 'tp', scatter_dimension=0, t...  36.2 us
    all_gather x1, waiting for transfers between devices, on_device(): whole = lax.all_gather(normed, 'tp', axis=0, tiled=True)  27.1 us
    dot_general x1, matrix products, on_device(): upward = jnp.dot(whole, up_full, preferred_element_type=jnp.float32)  11.9 us
    dot_general x1, matrix products, on_device(): terms = jnp.dot(act, down_full, preferred_element_type=jnp.float32)  11.8 us
  transfers between devices with their start and end apart: 6, of which 5 were waited for; matrix products, arithmetic and copies ran while one was open for 3% of the time, Pallas kernels for 0%

commit v1 on v0

--- a/solution.py
+++ b/solution.py
@@ -88,7 +88,12 @@
         tiled=True,
     ).astype(jnp.float32)
     normed = layer_norm(deep_alpha * residual.astype(jnp.float32) + mix, gains[0], biases[0])
-    whole = lax.all_gather(normed, "tp", axis=0, tiled=True)
+    ring = [normed]
+    for hop in range(3):
+        ring.append(lax.ppermute(ring[-1], "tp", [(dev, (dev + 1) % 4) for dev in range(4)]))
+    whole = jnp.roll(
+        jnp.concatenate(ring[::-1], axis=0), (lax.axis_index("tp") + 1) * ring[0].shape[0], axis=0
+    )
     upward = jnp.dot(whole, up_full, preferred_element_type=jnp.float32)
     act = jnp.square(jax.nn.relu(upward)).astype(jnp.bfloat16)
     terms = jnp.dot(act, down_full, preferred_element_type=jnp.float32)

time: 409 us -> 350 us (0.86)
  waiting for transfers between devices: 344 us -> 273 us
  local copies, waits for them, and re-layouts: 4.69 us -> 18.1 us
    all_gather x1, waiting for transfers between devices: 127 us -> 38.1 us  [on_device(): lax.all_gather(up_weight, 'sp', axis=0, tiled=True)]
    ppermute x0 -> x3, waiting for transfers between devices: none -> 34.6 us  [on_device(): lax.ppermute(ring[-1], 'tp', [(dev, (dev + 1) % 4) for dev in range(4)])]
    all_gather x1 -> x0, waiting for transfers between devices: 27.1 us -> none  [on_device(): whole = lax.all_gather(normed, 'tp', axis=0, tiled=True)]
    dot_general x1 -> x0, matrix products: 11.9 us -> none  [on_device(): upward = jnp.dot(whole, up_full, preferred_element_type=jnp.float32)]
    all_gather x1, waiting for transfers between devices: 113 us -> 125 us  [on_device(): lax.all_gather(down_weight, 'sp', axis=1, tiled=True)]
    unnamed x22 -> x27, local copies, waits for them, and re-layouts: 2 us -> 12.6 us
    dot_general x1, matrix products: 11.8 us -> 21.5 us  [on_device(): terms = jnp.dot(act, down_full, preferred_element_type=jnp.float32)]
  transfers between devices with their start and end apart: 6 -> 8, of which waited for: 5 -> 7; matrix products, arithmetic and copies ran while one was open for 3% -> 5% of each run, Pallas kernels for 0% -> 0%
where the time goes in v1:
time: 350 us; the launch traced here: 349 us
  waiting for transfers between devices  273 us (78%)
  matrix products  27.8 us (8%)
  local copies, waits for them, and re-layouts  18.1 us (5%)
  between operations  15.1 us (4%)
  other arithmetic  9.79 us (3%)
  starting transfers between devices  5.7 us (2%)
    all_gather x1, waiting for transfers between devices, on_device(): lax.all_gather(down_weight, 'sp', axis=1, tiled=True)  125 us
    all_gather x1, waiting for transfers between devices, on_device(): lax.all_gather(up_weight, 'sp', axis=0, tiled=True)  38.1 us
    reduce_scatter x1, waiting for transfers between devices, on_device(): lax.psum_scatter(jnp.dot(attended, out_weight, preferred_element_type=jnp...  37.7 us
    reduce_scatter x1, waiting for transfers between devices, on_device(): lax.psum_scatter(terms.astype(jnp.bfloat16), 'tp', scatter_dimension=0, t...  36.2 us
    ppermute x3, waiting for transfers between devices, on_device(): lax.ppermute(ring[-1], 'tp', [(dev, (dev + 1) % 4) for dev in range(4)])  34.6 us
    dot_general x1, matrix products, on_device(): terms = jnp.dot(act, down_full, preferred_element_type=jnp.float32)  21.5 us
    unnamed x27, local copies, waits for them, and re-layouts  12.6 us
  transfers between devices with their start and end apart: 8, of which 7 were waited for; matrix products, arithmetic and copies ran while one was open for 5% of the time, Pallas kernels for 0%

profile of v1, /device:TPU:0, one launch (start us, length us, event | category | flops | bytes accessed | tf_op | source)
XLA Modules:
  0.0 349.1 jit_solution(1018518502505887996)
XLA Ops:
  9.0 5.5 %collective-permute-start = (bf16[2,128,128]{2,1,0:T(8,128)(2,1)}, bf16[2,128,128]{2,1,0:T(8,128)(2,1)}, u32[]{:S(2)}, u32[]{:S(2)}) collective-permute-start(bf16[2,128,128]{2,1,0:T(8,128)(2,1)} %pad_maximum_fusion.2), channel_id=1, source_target_pairs={{0,4},{4,8},{8,12},{12,16},{16,20},{20,24},{24,28},{1,5},{5,9},{9,... | collective-permute-start | bytes 196616 | tf_op jit(solution)/shard_map/ppermute | solution.py:17
  15.0 2.0 reshape.206
  18.8 1.3 copy-done.4
  20.8 2.2 fusion.3
  23.4 3.5 convolution_convert_fusion.1
  28.2 37.7 %reduce-scatter.3.cloned.1.call-done = bf16[192,2048]{1,0:T(8,128)(2,1)} async-done(((bf16[768,2048]{1,0:T(8,128)(2,1)}), bf16[192,2048]{1,0:T(8,128)(2,1)}) %reduce-scatter.3.cloned.1.call-update) | async-done | bytes 786448 | tf_op jit(solution)/shard_map/reduce_scatter | solution.py:84
  65.9 1.5 fusion.4
  67.4 1.6 multiply_reduce_fusion.1
  69.6 11.4 %collective-permute-done.1 = bf16[192,2048]{1,0:T(8,128)(2,1)S(1)} collective-permute-done((bf16[192,2048]{1,0:T(8,128)(2,1)S(1)}, bf16[192,2048]{1,0:T(8,128)(2,1)S(1)}, u32[]{:S(2)}, u32[]{:S(2)}) %collective-permute-start.1) | collective-permute-done | bytes 786464 | tf_op jit(solution)/shard_map/ppermute | solution.py:93
  81.0 11.5 %collective-permute-done.2 = bf16[192,2048]{1,0:T(8,128)(2,1)} collective-permute-done((bf16[192,2048]{1,0:T(8,128)(2,1)S(1)}, bf16[192,2048]{1,0:T(8,128)(2,1)}, u32[]{:S(2)}, u32[]{:S(2)}) %collective-permute-start.2) | collective-permute-done | bytes 786464 | tf_op jit(solution)/shard_map/ppermute | solution.py:93
  92.5 11.7 %collective-permute-done.3 = bf16[192,2048]{1,0:T(8,128)(2,1)} collective-permute-done((bf16[192,2048]{1,0:T(8,128)(2,1)}, bf16[192,2048]{1,0:T(8,128)(2,1)}, u32[]{:S(2)}, u32[]{:S(2)}) %collective-permute-start.3) | collective-permute-done | bytes 786464 | tf_op jit(solution)/shard_map/ppermute | solution.py:93
  104.2 2.1 constant_dynamic-update-slice_fusion.7
  106.3 2.1 constant_dynamic-update-slice_fusion.6
  110.3 2.1 constant_dynamic-update-slice_fusion.3
  112.4 2.1 constant_dynamic-update-slice_fusion.2
  114.5 1.0 constant_dynamic-update-slice_fusion.1
  115.5 1.0 constant_dynamic-update-slice_fusion
  116.5 38.1 %all-gather.3.cloned.1.call-done = bf16[2048,2048]{1,0:T(8,128)(2,1)} async-done(((bf16[256,2048]{1,0:T(8,128)(2,1)}), bf16[2048,2048]{1,0:T(8,128)(2,1)}) %all-gather.3.cloned.1.call-update) | async-done | bytes 8388624 | tf_op jit(solution)/shard_map/all_gather | solution.py:77
  154.6 124.8 %all-gather.5.cloned.1.call-done = bf16[2048,2048]{1,0:T(8,128)(2,1)} async-done(((bf16[2048,256]{1,0:T(8,128)(2,1)}), bf16[2048,2048]{1,0:T(8,128)(2,1)}) %all-gather.5.cloned.1.call-update) | async-done | bytes 8388624 | tf_op jit(solution)/shard_map/all_gather | solution.py:78
  279.5 21.5 %convolution_convert_fusion = bf16[768,2048]{1,0:T(8,128)(2,1)} fusion(bf16[2048,2048]{1,0:T(8,128)(2,1)} %all-gather.5.cloned.1.call-done, bf16[2048,2048]{1,0:T(8,128)(2,1)} %all-gather.3.cloned.1.call-done, bf16[1536,2048]{1,0:T(8,128)(2,1)} %constant_dynamic-update-slice_fusion, s32[]{:T(128)S(6)} %select_n.19), kind=kOutput, calls=%fused_computation.1 | convolution fusion | flops 12891193344 | bytes 23068676 | tf_op jit(solution)/shard_map/dot_general | solution.py:99
  301.0 36.2 %reduce-scatter.5.cloned.1.call-done = bf16[192,2048]{1,0:T(8,128)(2,1)} async-done(((bf16[768,2048]{1,0:T(8,128)(2,1)}), bf16[192,2048]{1,0:T(8,128)(2,1)}) %reduce-scatter.5.cloned.1.call-update) | async-done | bytes 786448 | tf_op jit(solution)/shard_map/reduce_scatter | solution.py:100
  337.2 1.5 fusion.5
  338.8 1.6 multiply_reduce_fusion
  340.3 1.3 add_convert_fusion
  (60 shorter events, 8.6 us)
Async XLA Ops:
  7.4 16.0 %copy-start = (bf16[384,2048]{1,0:T(8,128)(2,1)S(1)}, bf16[384,2048]{1,0:T(8,128)(2,1)}, u32[]{:S(2)}) copy-start(bf16[384,2048]{1,0:T(8,128)(2,1)} %param.15) | copy-start | bytes 4718596
  7.4 10.7 %copy-start.6 = (bf16[768,128]{1,0:T(8,128)(2,1)S(1)}, bf16[768,128]{1,0:T(8,128)(2,1)}, u32[]{:S(2)}) copy-start(bf16[768,128]{1,0:T(8,128)(2,1)} %param.11) | copy-start | bytes 589828
  7.4 9.7 %copy-start.5 = (bf16[768,128]{1,0:T(8,128)(2,1)S(1)}, bf16[768,128]{1,0:T(8,128)(2,1)}, u32[]{:S(2)}) copy-start(bf16[768,128]{1,0:T(8,128)(2,1)} %param.12) | copy-start | bytes 589828
  7.4 58.5 %reduce-scatter.3.cloned.1.call-start = ((), (), s32[]{:S(2)}) async-start(), calls=%async_computation.2 | async-start | bytes 3932160 | tf_op jit(solution)/shard_map/reduce_scatter | solution.py:84
  9.0 8.3 %collective-permute-start = (bf16[2,128,128]{2,1,0:T(8,128)(2,1)}, bf16[2,128,128]{2,1,0:T(8,128)(2,1)}, u32[]{:S(2)}, u32[]{:S(2)}) collective-permute-start(bf16[2,128,128]{2,1,0:T(8,128)(2,1)} %pad_maximum_fusion.2), channel_id=1, source_target_pairs={{0,4},{4,8},{8,12},{12,16},{16,20},{20,24},{24,28},{1,5},{5,9},{9,... | collective-permute-start | bytes 196616 | tf_op jit(solution)/shard_map/ppermute | solution.py:17
  18.0 0.7 copy-start.9
  18.7 1.4 copy-start.4
  26.9 1.3 copy-start.7
  26.9 1.3 copy-start.8
  26.9 39.0 %copy-start.1 = (bf16[192,2048]{1,0:T(8,128)(2,1)S(1)}, bf16[192,2048]{1,0:T(8,128)(2,1)}, u32[]{:S(2)}) copy-start(bf16[192,2048]{1,0:T(8,128)(2,1)} %param.13) | copy-start | bytes 2359300
  26.9 127.7 %all-gather.3.cloned.1.call-start = ((), (), s32[]{:S(2)}) async-start(), calls=%async_computation.3 | async-start | bytes 9437184 | tf_op jit(solution)/shard_map/all_gather | solution.py:77
  27.5 252.0 %all-gather.5.cloned.1.call-start = ((), (), s32[]{:S(2)}) async-start(), calls=%async_computation.4 | async-start | bytes 9437184 | tf_op jit(solution)/shard_map/all_gather | solution.py:78
  28.1 309.1 %reduce-scatter.5.cloned.1.call-start = ((), (), s32[]{:S(2)}) async-start(), calls=%async_computation.5 | async-start | bytes 3932160 | tf_op jit(solution)/shard_map/reduce_scatter | solution.py:100
  65.9 3.1 copy-start.2
  69.5 11.5 %collective-permute-start.1 = (bf16[192,2048]{1,0:T(8,128)(2,1)S(1)}, bf16[192,2048]{1,0:T(8,128)(2,1)S(1)}, u32[]{:S(2)}, u32[]{:S(2)}) collective-permute-start(bf16[192,2048]{1,0:T(8,128)(2,1)S(1)} %add_convert_fusion.1), channel_id=1, source_target_pairs={{0,1},{1,2},{2,3},{3,0},{4,5},{5,6},{6,7},{7,4},{8,9},{9,10},{10,1... | collective-permute-start | bytes 2359304 | tf_op jit(solution)/shard_map/ppermute | solution.py:93
  81.0 11.5 %collective-permute-start.2 = (bf16[192,2048]{1,0:T(8,128)(2,1)S(1)}, bf16[192,2048]{1,0:T(8,128)(2,1)}, u32[]{:S(2)}, u32[]{:S(2)}) collective-permute-start(bf16[192,2048]{1,0:T(8,128)(2,1)S(1)} %collective-permute-done.1), channel_id=1, source_target_pairs={{0,1},{1,2},{2,3},{3,0},{4,5},{5,6},{6,7},{7,4},{8,9},{9,10},{10,1... | collective-permute-start | bytes 2359304 | tf_op jit(solution)/shard_map/ppermute | solution.py:93
  92.5 11.7 %collective-permute-start.3 = (bf16[192,2048]{1,0:T(8,128)(2,1)}, bf16[192,2048]{1,0:T(8,128)(2,1)}, u32[]{:S(2)}, u32[]{:S(2)}) collective-permute-start(bf16[192,2048]{1,0:T(8,128)(2,1)} %collective-permute-done.2), channel_id=1, source_target_pairs={{0,1},{1,2},{2,3},{3,0},{4,5},{5,6},{6,7},{7,4},{8,9},{9,10},{10,1... | collective-permute-start | bytes 2359304 | tf_op jit(solution)/shard_map/ppermute | solution.py:93
  337.2 3.1 copy-start.3
Sparse Core Ops, SparseCore 0:
  27.0 38.7 reduce-scatter.2
  301.1 36.0 reduce-scatter.4
Sparse Core Ops, SparseCore 1:
  29.5 125.0 all-gather.2
  156.5 122.9 all-gather.4
